TPU v7x, 1024 devices: a whole 8x8x8 slice. The times are simulated.
1024 devices in a mesh: row: 64 (over z, y), col: 16 (over x, core).
Axes of the slice: x: 8, y: 8, z: 8, core: 2. Of those that a mesh axis runs over, the one named last changes fastest.
Arguments:
- tokens: bfloat16 [2, 256, 64, 2048], P(None, 'row', 'col'), may hold values from -6 to 6
- norm_gain: bfloat16 [2048], replicated, may hold values from 0.099609375 to 1.8984375
- w_mix_in: bfloat16 [2048, 1024], replicated, may hold values from -0.125 to 0.125
- w_mix_out: bfloat16 [1024, 2048], replicated, may hold values from -0.1875 to 0.1875
Outputs:
- mixed_tokens: bfloat16 [2, 64, 256, 2048], P(None, 'row', 'col')
All inputs are finite; a program needn't handle non-finite values.
Results may differ from a plain program's by a relative error of at most 0.013.
Values may be sent and summed in bfloat16 or wider, within the bound.
No kernel may reach another device: no remote copies, remote signals or barrier semaphores. Data moves between devices by JAX's collectives and lax.ppermute only.
A program may use at most 32 MiB of HBM per device.

v0:
```python
import math

import jax
import jax.numpy as jnp
from jax import lax
from jax.sharding import PartitionSpec as P

G = 128


EPS = 1e-06


def as_sent(x):

    def short(part):
        return part.astype(jnp.bfloat16) if part.dtype == jnp.float32 else part

    return jax.tree.map(short, x)


def phase_table(count_first, count_second, period, first_start):
    first_index = lax.iota(jnp.int32, count_first) + first_start
    second_index = lax.iota(jnp.int32, count_second)
    turn_count = first_index[:, None] * second_index[None, :] % period
    phases = turn_count.astype(jnp.float32) * (2.0 * math.pi / period)
    return (jnp.cos(phases), jnp.sin(phases))


def packed_table(group_width):
    source = lax.iota(jnp.int32, group_width)
    column = lax.iota(jnp.int32, group_width)
    pair_index = column // 2
    frequency = jnp.where(column == 1, group_width // 2, pair_index)
    use_sine = (column % 2 == 1) & (pair_index > 0)
    turn_count = source[:, None] * frequency[None, :] % group_width
    phases = turn_count.astype(jnp.float32) * (2.0 * math.pi / group_width)
    return jnp.where(use_sine[None, :], jnp.sin(phases), jnp.cos(phases)) / math.sqrt(group_width)


def body(tokens, norm_gain, w_mix_in, w_mix_out):
    seq_count, rows_here, cols_here, width = tokens.shape
    row_devices = lax.axis_size("row")
    col_devices = lax.axis_size("col")
    len_first = rows_here * row_devices
    len_second = cols_here * col_devices
    seq_length = len_first * len_second
    features = w_mix_in.shape[1]
    share = features // row_devices
    groups = features // G
    scaled = tokens.astype(jnp.float32)
    mean_square = jnp.mean(scaled * scaled, axis=-1, keepdims=True)
    normed = (scaled * lax.rsqrt(mean_square + EPS) * norm_gain.astype(jnp.float32)).astype(
        jnp.bfloat16
    )
    mixing_in = jnp.dot(
        normed.reshape(-1, width), w_mix_in, preferred_element_type=jnp.float32
    ).astype(jnp.bfloat16)
    grouped = mixing_in.astype(jnp.float32).reshape(seq_count, rows_here, cols_here, groups, G)
    first_cos, first_sin = phase_table(len_first, len_first, len_first, 0)
    first_cos = first_cos / math.sqrt(len_first)
    first_sin = first_sin / math.sqrt(len_first)
    col_start = lax.axis_index("col") * cols_here
    twist_cos, twist_sin = phase_table(cols_here, len_first, seq_length, col_start)
    twist_cos = twist_cos[None, :, None, :]
    twist_sin = twist_sin[None, :, None, :]
    packed = jnp.einsum("sabgc,cm->sabgm", grouped, packed_table(G))
    packed = packed.reshape(seq_count, rows_here, cols_here, features)
    turned = jnp.transpose(
        lax.all_to_all(
            packed.astype(jnp.bfloat16), "row", split_axis=3, concat_axis=1, tiled=True
        ).astype(packed.dtype),
        (0, 2, 3, 1),
    )
    real_out = jnp.einsum("njft,tk->njfk", turned, first_cos)
    imag_out = -jnp.einsum("njft,tk->njfk", turned, first_sin)
    spec_real = real_out * twist_cos + imag_out * twist_sin
    spec_imag = imag_out * twist_cos - real_out * twist_sin
    second_cos, second_sin = phase_table(len_second, len_second, len_second, 0)
    second_cos = second_cos / math.sqrt(len_second)
    second_sin = second_sin / math.sqrt(len_second)
    row_start = lax.axis_index("row") * share
    pair_global = row_start // 2 + lax.iota(jnp.int32, share // 2)
    head_pair = (pair_global % (G // 2) == 0)[:, None]
    real_in = lax.all_to_all(
        as_sent(spec_real), "col", split_axis=3, concat_axis=1, tiled=True
    ).astype(spec_real.dtype)
    imag_in = lax.all_to_all(
        as_sent(spec_imag), "col", split_axis=3, concat_axis=1, tiled=True
    ).astype(spec_imag.dtype)
    real_turned = jnp.transpose(real_in, (0, 3, 2, 1))
    imag_turned = jnp.transpose(imag_in, (0, 3, 2, 1))
    real_out = jnp.einsum("nqft,tk->nqfk", real_turned, second_cos) + jnp.einsum(
        "nqft,tk->nqfk", imag_turned, second_sin
    )
    imag_out = jnp.einsum("nqft,tk->nqfk", imag_turned, second_cos) - jnp.einsum(
        "nqft,tk->nqfk", real_turned, second_sin
    )
    out_shape = real_out.shape
    pair_shape = out_shape[:2] + (share // 2, 2, out_shape[3])
    real_pairs = real_out.reshape(pair_shape)
    imag_pairs = imag_out.reshape(pair_shape)
    even_real = real_pairs[:, :, :, 0, :]
    odd_real = real_pairs[:, :, :, 1, :]
    odd_imag = imag_pairs[:, :, :, 1, :]
    low_freq = jnp.where(head_pair, even_real, even_real + odd_imag)
    high_freq = jnp.where(head_pair, odd_real, even_real - odd_imag)
    joined = jnp.stack([low_freq, high_freq], axis=3).reshape(out_shape).astype(jnp.bfloat16)
    mixed = jnp.transpose(joined, (0, 3, 1, 2))
    piece = lax.all_to_all(mixed, "row", split_axis=1, concat_axis=3, tiled=True)
    paired = piece.reshape(piece.shape[:-1] + (groups, G // 2, 2))
    low_freq = paired[..., 0]
    high_freq = paired[..., 1]
    natural = jnp.concatenate(
        [low_freq, high_freq[..., :1], jnp.flip(high_freq[..., 1:], axis=-1)], axis=-1
    )
    project_piece = natural.reshape(piece.shape)
    flat = project_piece.reshape(-1, features)
    output = jnp.dot(flat, w_mix_out, preferred_element_type=jnp.float32).astype(jnp.bfloat16)
    return output.reshape(project_piece.shape[:-1] + (width,))


def solution(mesh):
    placed = (P(None, "row", "col", None), P(), P(), P())
    return jax.shard_map(
        body, mesh=mesh, in_specs=placed, out_specs=P(None, "row", "col", None), check_vma=False
    )
```

profile of v0, /device:TPU:1, one launch (start us, length us, event | category | flops | bytes accessed | tf_op | source)
XLA Modules:
  0.0 114.2 jit_solution(9198953448739858335)
XLA Ops:
  0.0 0.7 convert_element_type.63
  0.7 1.1 fusion.1
  1.8 1.0 fusion.3
  2.9 3.0 %fusion = bf16[4,8,8,128]{3,1,2,0:T(8,128)(2,1)S(1)} fusion(bf16[32,2048]{1,0:T(8,128)(2,1)S(1)} %reshape.114, bf16[2048,1024]{1,0:T(8,128)(2,1)} %param.6), kind=kOutput, calls=%fused_computation.6 | convolution fusion | flops 134250496 | bytes 4390912 | tf_op jit(solution)/shard_map/dot_general | solution.py:56
  6.3 1.5 %copy.39 = bf16[2,4,4,8,128]{2,1,0,4,3:T(4,128)(2,1)S(1)} copy(bf16[2,4,4,8,128]{4,3,2,1,0:T(8,128)(2,1)S(1)} %convolution_convert_fusion.2) | data formatting | bytes 131072 | tf_op jit(solution)/shard_map/convert_element_type | solution.py:71
  7.8 4.6 %reshape.125 = bf16[64,2,256]{2,1,0:T(2,128)(2,1)} reshape(bf16[1024,2,4,4]{3,2,1,0:T(4,128)(2,1)S(1)} %bitcast.100) | data formatting | bytes 131072
  12.5 23.9 %all-to-all-start = ((bf16[64,2,256]{2,1,0:T(2,128)(2,1)}), bf16[64,2,256]{2,1,0:T(2,128)(2,1)S(1)}, u32[]{:S(2)}, u32[]{:S(2)}) async-start(bf16[64,2,256]{2,1,0:T(2,128)(2,1)} %reshape.125), calls=%async_computation | async-start | bytes 131072 | tf_op jit(solution)/shard_map/all_to_all | solution.py:70
  36.6 10.9 %all-to-all-done = bf16[64,2,256]{2,1,0:T(2,128)(2,1)S(1)} async-done(((bf16[64,2,256]{2,1,0:T(2,128)(2,1)}), bf16[64,2,256]{2,1,0:T(2,128)(2,1)S(1)}, u32[]{:S(2)}, u32[]{:S(2)}) %all-to-all-start) | async-done | bytes 65568 | tf_op jit(solution)/shard_map/all_to_all | solution.py:70
  47.5 4.5 %reshape.126 = bf16[1024,2,4,4]{3,2,1,0:T(4,128)(2,1)S(1)} reshape(bf16[64,2,256]{2,1,0:T(2,128)(2,1)S(1)} %all-to-all-done) | data formatting | bytes 131072
  52.0 4.8 %copy.40 = bf16[2,4,4,64,16]{4,3,2,1,0:T(8,128)(2,1)S(1)} copy(bf16[2,4,4,64,16]{2,1,0,4,3:T(4,128)(2,1)S(1)} %bitcast.99) | data formatting | bytes 131072 | tf_op jit(solution)/shard_map/all_to_all | solution.py:70
  57.4 1.1 convolution_negate_fusion
  58.5 1.1 subtract_convert_fusion
  60.0 1.2 %reshape.129 = bf16[16,2,1024]{2,1,0:T(2,128)(2,1)} reshape(bf16[256,2,4,16]{3,2,1,0:T(4,128)(2,1)S(1)} %bitcast.104) | data formatting | bytes 131072
  61.2 8.9 %all-to-all-start.2 = ((bf16[16,2,1024]{2,1,0:T(2,128)(2,1)}), bf16[16,2,1024]{2,1,0:T(2,128)(2,1)S(1)}, u32[]{:S(2)}, u32[]{:S(2)}) async-start(bf16[16,2,1024]{2,1,0:T(2,128)(2,1)} %reshape.129), calls=%async_computation.2 | async-start | bytes 131072 | tf_op jit(solution)/shard_map/all_to_all | solution.py:88
  70.4 1.2 %reshape.127 = bf16[16,2,1024]{2,1,0:T(2,128)(2,1)} reshape(bf16[256,2,4,16]{3,2,1,0:T(4,128)(2,1)S(1)} %bitcast.105) | data formatting | bytes 131072
  71.6 6.3 %all-to-all-done.2 = bf16[16,2,1024]{2,1,0:T(2,128)(2,1)S(1)} async-done(((bf16[16,2,1024]{2,1,0:T(2,128)(2,1)}), bf16[16,2,1024]{2,1,0:T(2,128)(2,1)S(1)}, u32[]{:S(2)}, u32[]{:S(2)}) %all-to-all-start.2) | async-done | bytes 65568 | tf_op jit(solution)/shard_map/all_to_all | solution.py:88
  77.8 3.6 %all-to-all-start.1 = ((bf16[16,2,1024]{2,1,0:T(2,128)(2,1)}), bf16[16,2,1024]{2,1,0:T(2,128)(2,1)S(1)}, u32[]{:S(2)}, u32[]{:S(2)}) async-start(bf16[16,2,1024]{2,1,0:T(2,128)(2,1)} %reshape.127), calls=%async_computation.1 | async-start | bytes 131072 | tf_op jit(solution)/shard_map/all_to_all | solution.py:85
  82.2 0.5 copy.28
  83.0 6.0 %all-to-all-done.1 = bf16[16,2,1024]{2,1,0:T(2,128)(2,1)S(1)} async-done(((bf16[16,2,1024]{2,1,0:T(2,128)(2,1)}), bf16[16,2,1024]{2,1,0:T(2,128)(2,1)S(1)}, u32[]{:S(2)}, u32[]{:S(2)}) %all-to-all-start.1) | async-done | bytes 65568 | tf_op jit(solution)/shard_map/all_to_all | solution.py:85
  89.8 0.5 copy.25
  92.0 0.5 copy.29
  93.0 14.9 %all_to_all.69 = bf16[64,2,256]{2,1,0:T(2,128)(2,1)S(1)} all-to-all(bf16[64,2,256]{2,1,0:T(2,128)(2,1)S(1)} %reshape.131), channel_id=1, replica_groups=mesh['row'=64,'col'=16] {'row'}, dimensions={0} | all-to-all | bytes 131072 | tf_op jit(solution)/shard_map/all_to_all | solution.py:110
  108.3 1.1 fusion.114
  110.5 3.7 %convolution_convert_fusion = bf16[32,2048]{1,0:T(8,128)(2,1)} fusion(bf16[1024,2048]{1,0:T(8,128)(2,1)} %param.7, bf16[4,8,8,128]{3,2,1,0:T(8,128)(2,1)S(1)} %bitcast.115), kind=kOutput, calls=%fused_computation | convolution fusion | flops 134283264 | bytes 4390912 | tf_op jit(solution)/shard_map/dot_general | solution.py:119
  (32 shorter events, 7.2 us)
Async XLA Ops:
  12.5 35.0 %all-to-all-start = ((bf16[64,2,256]{2,1,0:T(2,128)(2,1)}), bf16[64,2,256]{2,1,0:T(2,128)(2,1)S(1)}, u32[]{:S(2)}, u32[]{:S(2)}) async-start(bf16[64,2,256]{2,1,0:T(2,128)(2,1)} %reshape.125), calls=%async_computation | async-start | bytes 131072 | tf_op jit(solution)/shard_map/all_to_all | solution.py:70
  61.2 16.6 %all-to-all-start.2 = ((bf16[16,2,1024]{2,1,0:T(2,128)(2,1)}), bf16[16,2,1024]{2,1,0:T(2,128)(2,1)S(1)}, u32[]{:S(2)}, u32[]{:S(2)}) async-start(bf16[16,2,1024]{2,1,0:T(2,128)(2,1)} %reshape.129), calls=%async_computation.2 | async-start | bytes 131072 | tf_op jit(solution)/shard_map/all_to_all | solution.py:88
  77.8 11.2 %all-to-all-start.1 = ((bf16[16,2,1024]{2,1,0:T(2,128)(2,1)}), bf16[16,2,1024]{2,1,0:T(2,128)(2,1)S(1)}, u32[]{:S(2)}, u32[]{:S(2)}) async-start(bf16[16,2,1024]{2,1,0:T(2,128)(2,1)} %reshape.127), calls=%async_computation.1 | async-start | bytes 131072 | tf_op jit(solution)/shard_map/all_to_all | solution.py:85
where the time goes:
time: 115 us; the launch traced here: 114 us
  starting transfers between devices  36.4 us (32%)
  local copies, waits for them, and re-layouts  25 us (22%)
  waiting for transfers between devices  23.2 us (20%)
  blocking collectives  14.9 us (13%)
  matrix products  10.6 us (9%)
  other arithmetic  3.81 us (3%)
    all_to_all x1, starting transfers between devices, body(): lax.all_to_all(packed.astype(jnp.bfloat16), 'row', split_axis=3, concat_a...  23.9 us
    all_to_all x1, blocking collectives, body(): lax.all_to_all(mixed, 'row', split_axis=1, concat_axis=3, tiled=True)  14.9 us
    unnamed x9, local copies, waits for them, and re-layouts  13.1 us
    all_to_all x1, waiting for transfers between devices, body(): lax.all_to_all(packed.astype(jnp.bfloat16), 'row', split_axis=3, concat_a...  10.9 us
    all_to_all x1, starting transfers between devices, body(): lax.all_to_all(as_sent(spec_imag), 'col', split_axis=3, concat_axis=1, ti...  8.88 us
    all_to_all x1, waiting for transfers between devices, body(): lax.all_to_all(as_sent(spec_imag), 'col', split_axis=3, concat_axis=1, ti...  6.25 us
    all_to_all x1, waiting for transfers between devices, body(): lax.all_to_all(as_sent(spec_real), 'col', split_axis=3, concat_axis=1, ti...  6.04 us
    all_to_all x3, local copies, waits for them, and re-layouts, body(): lax.all_to_all(packed.astype(jnp.bfloat16), 'row', split_axis=3, concat_a...  5.37 us
  transfers between devices with their start and end apart: 3, of which 3 were waited for; matrix products, arithmetic and copies ran while one was open for 3% of the time, Pallas kernels for 0%

commit v1 on v0

v1 whole, which is shorter than its diff:
```python
import math

import jax
import jax.numpy as jnp
import numpy as np
from jax import lax
from jax.experimental import pallas as pl
from jax.experimental.pallas import tpu as pltpu
from jax.sharding import PartitionSpec as P

D = 2048
F = 1024
G = 128
GROUPS = F // G
SEQS = 2
ROW = 64
COL = 16
A = 4
B = 4
LEN1 = ROW * A
LEN2 = COL * B
LENGTH = LEN1 * LEN2
EPS = 1e-06
IN_CHUNKS = 4
OUT_CHUNKS = 8
bf16 = jnp.bfloat16
f32 = jnp.float32


def channel_table():
    c = np.arange(G)[None, :]
    r = np.arange(ROW)[:, None]
    cos = np.cos(2 * np.pi * (c * r % G) / G)
    sin = np.sin(2 * np.pi * (c * r % G) / G)
    sin[0] = np.cos(np.pi * np.arange(G))
    return np.concatenate([cos, sin], 0)


def first_tables():
    k1 = np.arange(LEN1)[:, None]
    phase = 2 * np.pi * (k1 * np.arange(LEN1)[None, :] % LEN1) / LEN1
    re, im = np.cos(phase) / math.sqrt(LEN1), -np.sin(phase) / math.sqrt(LEN1)
    straight = np.stack([re, im], 1).reshape(2 * LEN1, LEN1)
    swapped = np.stack([im, -re], 1).reshape(2 * LEN1, LEN1)
    return straight, swapped


def twist_tables():
    k1 = np.repeat(np.arange(LEN1), 2)
    b = np.arange(128) % B
    q = 2 * np.pi * k1[:, None] * b[None, :] / LENGTH
    p = 2 * np.pi * k1[None, :] * (B * np.arange(COL))[:, None] / LENGTH
    pt = np.zeros((COL, 8, 2 * LEN1))
    pt[:, 0] = np.cos(p)
    pt[:, 1] = np.sin(p)
    return np.cos(q), np.sin(q), pt


def second_table():
    k2 = np.arange(LEN2)[:, None]
    phase = 2 * np.pi * (k2 * np.arange(LEN2)[None, :] % LEN2) / LEN2
    cos, sin = np.cos(phase) / math.sqrt(LEN2), np.sin(phase) / math.sqrt(LEN2)
    real = np.stack([cos, sin], 2).reshape(LEN2, 2 * LEN2)
    imag = np.stack([-sin, cos], 2).reshape(LEN2, 2 * LEN2)
    return np.concatenate([real, imag], 0)


def order_table():
    table = np.zeros((ROW, 2, SEQS, SEQS, G))
    for r in range(ROW):
        for s in range(SEQS):
            table[r, 0, s, s, r] = 1
            table[r, 1, s, s, G - r if r else G // 2] = 1
    return table.reshape(4 * ROW, SEQS * G)


def front_kernel(x_ref, gain_ref, table_ref, w_hbm, y_ref, w_ref, rows_ref, send_ref, sems):
    width = F // IN_CHUNKS
    copies = []
    for i in range(IN_CHUNKS):
        cols = pl.ds(i * width, width)
        copies.append(pltpu.make_async_copy(w_hbm.at[:, cols], w_ref.at[:, cols], sems.at[i]))
        copies[-1].start()
    for a in range(A):
        for s in range(SEQS):
            rows_ref[pl.ds(8 * a + 4 * s, 4), :] = x_ref[s, a].astype(f32)
    x = rows_ref[...]
    mean_square = jnp.mean(x * x, axis=-1, keepdims=True)
    normed = (x * lax.rsqrt(mean_square + EPS) * gain_ref[...].astype(f32)).astype(bf16)
    parts = []
    for i in range(IN_CHUNKS):
        copies[i].wait()
        parts.append(jnp.dot(normed, w_ref[:, i * width : (i + 1) * width], preferred_element_type=f32))
    per = width // G
    table = table_ref[...]
    lane = lax.broadcasted_iota(jnp.int32, (ROW, 128), 1)
    first = (lane // 8) % 2 == 0
    for a in range(A):
        blocks = []
        for g in range(GROUPS):
            block = parts[g // per][8 * a : 8 * a + 8, (g % per) * G : (g % per + 1) * G]
            blocks += [block, block]
        stacked = jnp.concatenate(blocks, 0).astype(bf16)
        both = lax.dot_general(table, stacked, (((1,), (1,)), ((), ())), preferred_element_type=f32)
        send_ref[pl.ds(a, ROW, stride=A), :] = jnp.where(first, both[:ROW], both[ROW:]) * (1 / math.sqrt(G))
    y_ref[...] = send_ref[...].astype(bf16)


def swap_sublane_lane(x, sub, lane_step):
    row_bit = (lax.broadcasted_iota(jnp.int32, x.shape, 1) // sub) % 2
    lane_bit = (lax.broadcasted_iota(jnp.int32, x.shape, 2) // lane_step) % 2
    up = pltpu.roll(pltpu.roll(x, 8 - sub, 1), lane_step, 2)
    down = pltpu.roll(pltpu.roll(x, sub, 1), 128 - lane_step, 2)
    return jnp.where(row_bit == lane_bit, x, jnp.where(lane_bit == 1, up, down))


def first_kernel(z_ref, straight_ref, swapped_ref, qc_ref, qs_ref, pt_ref, o_ref):
    c = lax.axis_index("col")
    z = z_ref[...]
    p = pt_ref[c].T
    step = 128
    for i in range(2 * LEN1 // step):
        rows = slice(i * step, (i + 1) * step)
        u = jnp.dot(straight_ref[rows, :], z, preferred_element_type=f32)
        v = jnp.dot(swapped_ref[rows, :], z, preferred_element_type=f32)
        pc, ps = p[rows, 0:1], p[rows, 1:2]
        qc, qs = qc_ref[rows, :], qs_ref[rows, :]
        turned = u * (pc * qc - ps * qs) + v * (ps * qc + pc * qs)
        turned = turned.reshape(step // 8, 8, 128)
        turned = swap_sublane_lane(turned, 2, 1)
        turned = swap_sublane_lane(turned, 4, 2).astype(bf16)
        for j in range(step // 8):
            n = i * (step // 8) + j
            o_ref[n // 4, :, (n % 4) * 128 : (n % 4 + 1) * 128] = turned[j]


def second_kernel(v_ref, table_ref, s_ref, send_ref):
    head = lax.axis_index("row") == 0
    both = jnp.dot(table_ref[...], v_ref[...], preferred_element_type=f32)
    lane = lax.broadcasted_iota(jnp.int32, (LEN2, 128), 1)
    l_bit, s_bit = (lane // 8) % 2, (lane // 4) % 2
    real_here = jnp.logical_or(l_bit == 0, head)
    tiles = []
    for h in range(4):
        cols = slice(128 * h, 128 * (h + 1))
        tiles.append(jnp.where(real_here, both[:LEN2, cols], both[LEN2:, cols]))
    for shift, bit, pairs in ((8, l_bit, ((0, 2), (1, 3))), (4, s_bit, ((0, 1), (2, 3)))):
        for i, j in pairs:
            low, high = tiles[i], tiles[j]
            tiles[i] = jnp.where(bit == 0, low, pltpu.roll(high, shift, 1))
            tiles[j] = jnp.where(bit == 1, high, pltpu.roll(low, 128 - shift, 1))
    for s in range(SEQS):
        even, odd = tiles[s], tiles[2 + s]
        send_ref[pl.ds(s, LEN2, stride=4), :] = jnp.where(head, even, even + odd)
        send_ref[pl.ds(2 + s, LEN2, stride=4), :] = jnp.where(head, odd, even - odd)
    s_ref[...] = send_ref[...].astype(bf16)


def final_kernel(x_ref, order_ref, w_hbm, o_ref, w_ref, sems):
    width = D // OUT_CHUNKS
    copies = []
    for i in range(OUT_CHUNKS):
        cols = pl.ds(i * width, width)
        copies.append(pltpu.make_async_copy(w_hbm.at[:, cols], w_ref.at[:, cols], sems.at[i]))
        copies[-1].start()
    turned = x_ref[...].astype(f32).T.astype(bf16)
    placed = jnp.dot(turned, order_ref[...], preferred_element_type=f32)
    columns = []
    for g in range(GROUPS):
        rows = slice(16 * g, 16 * (g + 1))
        columns.append(jnp.concatenate([placed[rows, :G], placed[rows, G:]], 0))
    flat = jnp.concatenate(columns, 1).astype(bf16)
    for i in range(OUT_CHUNKS):
        copies[i].wait()
        cols = slice(i * width, (i + 1) * width)
        o_ref[:, cols] = jnp.dot(flat, w_ref[:, cols], preferred_element_type=f32).astype(bf16)


VMEM = pl.BlockSpec(memory_space=pltpu.VMEM)
ANY = pl.BlockSpec(memory_space=pl.ANY)


def body(tokens, norm_gain, w_mix_in, w_mix_out):
    def const(x, kind):
        return jnp.asarray(x.astype(kind))

    straight, swapped = first_tables()
    qc, qs, pt = twist_tables()
    y = pl.pallas_call(
        front_kernel,
        out_shape=jax.ShapeDtypeStruct((ROW * A, 128), bf16),
        in_specs=[VMEM, VMEM, VMEM, ANY],
        out_specs=VMEM,
        scratch_shapes=[
            pltpu.VMEM((D, F), bf16),
            pltpu.VMEM((32, D), f32),
            pltpu.VMEM((ROW * A, 128), f32),
            pltpu.SemaphoreType.DMA((IN_CHUNKS,)),
        ],
        name="front",
    )(tokens, norm_gain.reshape(1, D), const(channel_table(), bf16), w_mix_in)
    z = lax.all_to_all(y, "row", split_axis=0, concat_axis=0, tiled=True)
    o = pl.pallas_call(
        first_kernel,
        out_shape=jax.ShapeDtypeStruct((COL, 8, 512), bf16),
        in_specs=[VMEM] * 6,
        out_specs=VMEM,
        name="first",
    )(z, const(straight, bf16), const(swapped, bf16), const(qc, f32), const(qs, f32), const(pt, f32))
    v = lax.all_to_all(o, "col", split_axis=0, concat_axis=0, tiled=True)
    s = pl.pallas_call(
        second_kernel,
        out_shape=jax.ShapeDtypeStruct((4 * ROW, 128), bf16),
        in_specs=[VMEM] * 2,
        out_specs=VMEM,
        scratch_shapes=[pltpu.VMEM((4 * ROW, 128), f32)],
        name="second",
    )(v.reshape(2 * LEN2, 512), const(second_table(), bf16))
    x = lax.all_to_all(s, "row", split_axis=0, concat_axis=0, tiled=True)
    out = pl.pallas_call(
        final_kernel,
        out_shape=jax.ShapeDtypeStruct((SEQS * 16, D), bf16),
        in_specs=[VMEM, VMEM, ANY],
        out_specs=VMEM,
        scratch_shapes=[pltpu.VMEM((F, D), bf16), pltpu.SemaphoreType.DMA((OUT_CHUNKS,))],
        name="final",
    )(x, const(order_table(), bf16), w_mix_out)
    return out.reshape(SEQS, 1, 16, D)


def solution(mesh):
    placed = (P(None, "row", "col", None), P(), P(), P())
    return jax.shard_map(
        body, mesh=mesh, in_specs=placed, out_specs=P(None, "row", "col", None), check_vma=False
    )
```

time: 115 us -> 85.3 us (0.74)
  blocking collectives: 14.9 us -> 69.5 us
  starting transfers between devices: 36.4 us -> 0 us
  local copies, waits for them, and re-layouts: 25 us -> 1.29 us
  waiting for transfers between devices: 23.2 us -> 0 us
  Pallas kernels: 0 us -> 14.1 us
  matrix products: 10.6 us -> 0 us
  other arithmetic: 3.81 us -> 0 us
    all_to_all x1 -> x3, blocking collectives: 14.9 us -> 69.5 us  [the longest x1 35.1 us: body(): z = lax.all_to_all(y, 'row', split_axis=0, concat_axis=0, tiled=True)]
    all_to_all x3 -> x0, starting transfers between devices: 36.4 us -> none  [the longest x1 23.9 us: body(): lax.all_to_all(packed.astype(jnp.bfloat16), 'row', split_axis=3, concat_a...]
    all_to_all x3 -> x0, waiting for transfers between devices: 23.2 us -> none  [the longest x1 10.9 us: body(): lax.all_to_all(packed.astype(jnp.bfloat16), 'row', split_axis=3, concat_a...]
    pallas_call x0 -> x4, Pallas kernels: none -> 14.1 us  [the longest x1 4.77 us: body(): pl.pallas_call(final_kernel, out_shape=jax.ShapeDtypeStruct((SEQS * 16, D...]
    unnamed x9 -> x0, local copies, waits for them, and re-layouts: 13.1 us -> none
    dot_general x9 -> x0, matrix products: 10.6 us -> none  [the longest x1 3.68 us: body(): jnp.dot(flat, w_mix_out, preferred_element_type=jnp.float32)]
    all_to_all x9 -> x0, local copies, waits for them, and re-layouts: 7.22 us -> none  [the longest x3 5.37 us: body(): lax.all_to_all(packed.astype(jnp.bfloat16), 'row', split_axis=3, concat_a...]
    convert_element_type x3 -> x0, local copies, waits for them, and re-layouts: 2.14 us -> none  [the longest x1 1.52 us: body(): packed.astype(jnp.bfloat16)]
  transfers between devices with their start and end apart: 3 -> 0, of which waited for: 3 -> 0; matrix products, arithmetic and copies ran while one was open for 3% -> 0% of each run, Pallas kernels for 0% -> 0%
where the time goes in v1:
time: 85.3 us; the launch traced here: 84.9 us
  blocking collectives  69.5 us (81%)
  Pallas kernels  14.1 us (17%)
  local copies, waits for them, and re-layouts  1.29 us (2%)
    all_to_all x1, blocking collectives, body(): z = lax.all_to_all(y, 'row', split_axis=0, concat_axis=0, tiled=True)  35.1 us
    all_to_all x1, blocking collectives, body(): v = lax.all_to_all(o, 'col', split_axis=0, concat_axis=0, tiled=True)  17.9 us
    all_to_all x1, blocking collectives, body(): x = lax.all_to_all(s, 'row', split_axis=0, concat_axis=0, tiled=True)  16.5 us
    pallas_call x1, Pallas kernels, body(): pl.pallas_call(final_kernel, out_shape=jax.ShapeDtypeStruct((SEQS * 16, D...  4.77 us
    pallas_call x1, Pallas kernels, body(): pl.pallas_call(front_kernel, out_shape=jax.ShapeDtypeStruct((ROW * A, 128...  4.57 us
    pallas_call x1, Pallas kernels, body(): pl.pallas_call(first_kernel, out_shape=jax.ShapeDtypeStruct((COL, 8, 512)...  2.84 us
    pallas_call x1, Pallas kernels, body(): pl.pallas_call(second_kernel, out_shape=jax.ShapeDtypeStruct((4 * ROW, 12...  1.88 us

profile of v1, /device:TPU:1, one launch (start us, length us, event | category | flops | bytes accessed | tf_op | source)
XLA Modules:
  0.0 84.9 jit_solution(15860178682500419021)
XLA Ops:
  0.0 1.3 %reshape.13.gain_ref = bf16[1,2048]{1,0:T(2,128)(2,1)} reshape(bf16[2048]{0:T(1024)(128)(2,1)} %param.13) | data formatting | bytes 8192 | tf_op jit(solution)/shard_map/reshape | solution.py:201
  1.3 4.6 %front.1 = bf16[256,128]{1,0:T(8,128)(2,1)} custom-call(bf16[2,4,4,2048]{3,2,1,0:T(4,128)(2,1)} %x_ref.1, bf16[1,2048]{1,0:T(2,128)(2,1)} %reshape.13.gain_ref, bf16[128,128]{1,0:T(8,128)(2,1)} %constant.16.clone.table_ref, bf16[2048,1024]{1,0:T(8,128)(2,1)} %w_hbm.2), custom_call_target="tpu_custom_call" | custom-call | tf_op jit(solution)/shard_map/front/pallas_call | solution.py:189
  5.9 35.1 %all_to_all.27 = bf16[64,4,128]{2,1,0:T(4,128)(2,1)} all-to-all(bf16[64,4,128]{2,1,0:T(4,128)(2,1)} %bitcast.9), channel_id=1, replica_groups=mesh['row'=64,'col'=16] {'row'}, dimensions={0} | all-to-all | bytes 131072 | tf_op jit(solution)/shard_map/all_to_all | solution.py:202
  41.0 2.8 %first.1 = bf16[16,8,512]{2,1,0:T(8,128)(2,1)} custom-call(bf16[256,128]{1,0:T(8,128)(2,1)} %bitcast.11, bf16[512,256]{1,0:T(8,128)(2,1)} %constant.17.clone.straight_ref, bf16[512,256]{1,0:T(8,128)(2,1)} %constant.18.clone.swapped_ref, f32[512,128]{1,0:T(8,128)} %constant.19.clone.qc_ref, f32[512,128]{1,0:T(8,128)} %constant.20.clone.qs_ref, ...), custom_call_target="tpu_custom_call" | custom-call | tf_op jit(solution)/shard_map/first/pallas_call | solution.py:203
  43.8 17.9 %all_to_all.28 = bf16[16,8,512]{2,1,0:T(8,128)(2,1)} all-to-all(bf16[16,8,512]{2,1,0:T(8,128)(2,1)} %first.1), channel_id=1, replica_groups=mesh['row'=64,'col'=16] {'col'}, dimensions={0} | all-to-all | bytes 262144 | tf_op jit(solution)/shard_map/all_to_all | solution.py:210
  61.7 1.9 %second.1 = bf16[256,128]{1,0:T(8,128)(2,1)} custom-call(bf16[128,512]{1,0:T(8,128)(2,1)} %bitcast.8, bf16[128,128]{1,0:T(8,128)(2,1)} %constant.22.clone.table_ref), custom_call_target="tpu_custom_call" | custom-call | tf_op jit(solution)/shard_map/second/pallas_call | solution.py:211
  63.6 16.5 %all_to_all.29 = bf16[64,4,128]{2,1,0:T(4,128)(2,1)} all-to-all(bf16[64,4,128]{2,1,0:T(4,128)(2,1)} %bitcast.12), channel_id=1, replica_groups=mesh['row'=64,'col'=16] {'row'}, dimensions={0} | all-to-all | bytes 131072 | tf_op jit(solution)/shard_map/all_to_all | solution.py:219
  80.1 4.8 %final.1 = bf16[32,2048]{1,0:T(8,128)(2,1)} custom-call(bf16[256,128]{1,0:T(8,128)(2,1)} %bitcast.10, bf16[256,256]{1,0:T(8,128)(2,1)} %constant.23.clone.order_ref, bf16[1024,2048]{1,0:T(8,128)(2,1)} %w_hbm.3), custom_call_target="tpu_custom_call" | custom-call | tf_op jit(solution)/shard_map/final/pallas_call | solution.py:220

commit v2 on v1

--- a/solution.py
+++ b/solution.py
@@ -45,15 +45,19 @@
     return straight, swapped
 
 
-def twist_tables():
-    k1 = np.repeat(np.arange(LEN1), 2)
-    b = np.arange(128) % B
-    q = 2 * np.pi * k1[:, None] * b[None, :] / LENGTH
-    p = 2 * np.pi * k1[None, :] * (B * np.arange(COL))[:, None] / LENGTH
-    pt = np.zeros((COL, 8, 2 * LEN1))
-    pt[:, 0] = np.cos(p)
-    pt[:, 1] = np.sin(p)
-    return np.cos(q), np.sin(q), pt
+def twist(shape, col, start):
+    row = lax.broadcasted_iota(jnp.int32, shape, 0) + start
+    lane = lax.broadcasted_iota(jnp.int32, shape, 1)
+    count = (row >> 1) * ((lane & (B - 1)) + B * col)
+    quarter = LENGTH // 4
+    quadrant = (count + quarter // 2) // quarter
+    x = (count - quadrant * quarter).astype(f32) * (2 * math.pi / LENGTH)
+    x2 = x * x
+    sin = x * (1 + x2 * (-1 / 6 + x2 * (1 / 120 + x2 * (-1 / 5040 + x2 * (1 / 362880)))))
+    cos = 1 + x2 * (-1 / 2 + x2 * (1 / 24 + x2 * (-1 / 720 + x2 * (1 / 40320))))
+    odd = (quadrant & 1) == 1
+    c, s = jnp.where(odd, sin, cos), jnp.where(odd, cos, sin)
+    return jnp.where(((quadrant + 1) & 2) == 2, -c, c), jnp.where((quadrant & 2) == 2, -s, s)
 
 
 def second_table():
@@ -74,24 +78,48 @@
     return table.reshape(4 * ROW, SEQS * G)
 
 
-def front_kernel(x_ref, gain_ref, table_ref, w_hbm, y_ref, w_ref, rows_ref, send_ref, sems):
+def front_kernel(
+    x_hbm, gain_hbm, table_hbm, w_hbm, straight_hbm, swapped_hbm,
+    y_ref, cos_ref, sin_ref, straight_ref, swapped_ref,
+    x_ref, gain_ref, table_ref, w_ref, rows_ref, send_ref, sems, w_sems,
+):
     width = F // IN_CHUNKS
+    x_copy = pltpu.make_async_copy(x_hbm, x_ref, sems.at[0])
+    x_copy.start()
+    gain_copy = pltpu.make_async_copy(gain_hbm, gain_ref, sems.at[4])
+    gain_copy.start()
     copies = []
     for i in range(IN_CHUNKS):
         cols = pl.ds(i * width, width)
-        copies.append(pltpu.make_async_copy(w_hbm.at[:, cols], w_ref.at[:, cols], sems.at[i]))
+        copies.append(pltpu.make_async_copy(w_hbm.at[:, cols], w_ref.at[:, cols], w_sems.at[i]))
         copies[-1].start()
+    table_copy = pltpu.make_async_copy(table_hbm, table_ref, sems.at[1])
+    table_copy.start()
+    others = [
+        pltpu.make_async_copy(straight_hbm, straight_ref, sems.at[2]),
+        pltpu.make_async_copy(swapped_hbm, swapped_ref, sems.at[3]),
+    ]
+    for copy in others:
+        copy.start()
+    col = lax.axis_index("col")
+    for i in range(8):
+        rows = slice(64 * i, 64 * (i + 1))
+        cos_ref[rows, :], sin_ref[rows, :] = twist((64, 128), col, 64 * i)
+    x_copy.wait()
     for a in range(A):
         for s in range(SEQS):
             rows_ref[pl.ds(8 * a + 4 * s, 4), :] = x_ref[s, a].astype(f32)
     x = rows_ref[...]
     mean_square = jnp.mean(x * x, axis=-1, keepdims=True)
-    normed = (x * lax.rsqrt(mean_square + EPS) * gain_ref[...].astype(f32)).astype(bf16)
+    gain_copy.wait()
+    gain = gain_ref[...].astype(f32).reshape(1, D)
+    normed = (x * lax.rsqrt(mean_square + EPS) * gain).astype(bf16)
     parts = []
     for i in range(IN_CHUNKS):
         copies[i].wait()
         parts.append(jnp.dot(normed, w_ref[:, i * width : (i + 1) * width], preferred_element_type=f32))
     per = width // G
+    table_copy.wait()
     table = table_ref[...]
     lane = lax.broadcasted_iota(jnp.int32, (ROW, 128), 1)
     first = (lane // 8) % 2 == 0
@@ -104,6 +132,8 @@
         both = lax.dot_general(table, stacked, (((1,), (1,)), ((), ())), preferred_element_type=f32)
         send_ref[pl.ds(a, ROW, stride=A), :] = jnp.where(first, both[:ROW], both[ROW:]) * (1 / math.sqrt(G))
     y_ref[...] = send_ref[...].astype(bf16)
+    for copy in others:
+        copy.wait()
 
 
 def swap_sublane_lane(x, sub, lane_step):
@@ -114,18 +144,14 @@
     return jnp.where(row_bit == lane_bit, x, jnp.where(lane_bit == 1, up, down))
 
 
-def first_kernel(z_ref, straight_ref, swapped_ref, qc_ref, qs_ref, pt_ref, o_ref):
-    c = lax.axis_index("col")
+def first_kernel(z_ref, straight_ref, swapped_ref, cos_ref, sin_ref, o_ref):
     z = z_ref[...]
-    p = pt_ref[c].T
     step = 128
     for i in range(2 * LEN1 // step):
         rows = slice(i * step, (i + 1) * step)
         u = jnp.dot(straight_ref[rows, :], z, preferred_element_type=f32)
         v = jnp.dot(swapped_ref[rows, :], z, preferred_element_type=f32)
-        pc, ps = p[rows, 0:1], p[rows, 1:2]
-        qc, qs = qc_ref[rows, :], qs_ref[rows, :]
-        turned = u * (pc * qc - ps * qs) + v * (ps * qc + pc * qs)
+        turned = u * cos_ref[rows, :] + v * sin_ref[rows, :]
         turned = turned.reshape(step // 8, 8, 128)
         turned = swap_sublane_lane(turned, 2, 1)
         turned = swap_sublane_lane(turned, 4, 2).astype(bf16)
@@ -156,13 +182,8 @@
     s_ref[...] = send_ref[...].astype(bf16)
 
 
-def final_kernel(x_ref, order_ref, w_hbm, o_ref, w_ref, sems):
+def final_kernel(x_ref, order_ref, w_ref, o_ref):
     width = D // OUT_CHUNKS
-    copies = []
-    for i in range(OUT_CHUNKS):
-        cols = pl.ds(i * width, width)
-        copies.append(pltpu.make_async_copy(w_hbm.at[:, cols], w_ref.at[:, cols], sems.at[i]))
-        copies[-1].start()
     turned = x_ref[...].astype(f32).T.astype(bf16)
     placed = jnp.dot(turned, order_ref[...], preferred_element_type=f32)
     columns = []
@@ -171,60 +192,92 @@
         columns.append(jnp.concatenate([placed[rows, :G], placed[rows, G:]], 0))
     flat = jnp.concatenate(columns, 1).astype(bf16)
     for i in range(OUT_CHUNKS):
-        copies[i].wait()
         cols = slice(i * width, (i + 1) * width)
         o_ref[:, cols] = jnp.dot(flat, w_ref[:, cols], preferred_element_type=f32).astype(bf16)
 
 
 VMEM = pl.BlockSpec(memory_space=pltpu.VMEM)
-ANY = pl.BlockSpec(memory_space=pl.ANY)
+HBM = pl.BlockSpec(memory_space=pltpu.HBM)
+
+
+def small(mib):
+    return pltpu.CompilerParams(vmem_limit_bytes=mib << 20)
+
+
+def in_hbm(x):
+    return pltpu.with_memory_space_constraint(x, pltpu.HBM)
+
+
+def shape(*dims, kind=bf16):
+    return jax.ShapeDtypeStruct(dims, kind)
 
 
 def body(tokens, norm_gain, w_mix_in, w_mix_out):
-    def const(x, kind):
-        return jnp.asarray(x.astype(kind))
+    def const(x):
+        return jnp.asarray(x.astype(bf16))
 
     straight, swapped = first_tables()
-    qc, qs, pt = twist_tables()
-    y = pl.pallas_call(
+    y, cos, sin, straight, swapped = pl.pallas_call(
         front_kernel,
-        out_shape=jax.ShapeDtypeStruct((ROW * A, 128), bf16),
-        in_specs=[VMEM, VMEM, VMEM, ANY],
-        out_specs=VMEM,
+        out_shape=[
+            shape(ROW * A, 128),
+            shape(2 * LEN1, 128, kind=f32),
+            shape(2 * LEN1, 128, kind=f32),
+            shape(2 * LEN1, LEN1),
+            shape(2 * LEN1, LEN1),
+        ],
+        in_specs=[HBM] * 6,
+        out_specs=[VMEM] * 5,
         scratch_shapes=[
+            pltpu.VMEM((SEQS, A, B, D), bf16),
+            pltpu.VMEM((D,), bf16),
+            pltpu.VMEM((G, G), bf16),
             pltpu.VMEM((D, F), bf16),
             pltpu.VMEM((32, D), f32),
             pltpu.VMEM((ROW * A, 128), f32),
+            pltpu.SemaphoreType.DMA((5,)),
             pltpu.SemaphoreType.DMA((IN_CHUNKS,)),
         ],
+        compiler_params=small(16),
         name="front",
-    )(tokens, norm_gain.reshape(1, D), const(channel_table(), bf16), w_mix_in)
+    )(
+        in_hbm(tokens),
+        in_hbm(norm_gain),
+        in_hbm(const(channel_table())),
+        in_hbm(w_mix_in),
+        in_hbm(const(straight)),
+        in_hbm(const(swapped)),
+    )
     z = lax.all_to_all(y, "row", split_axis=0, concat_axis=0, tiled=True)
     o = pl.pallas_call(
         first_kernel,
-        out_shape=jax.ShapeDtypeStruct((COL, 8, 512), bf16),
-        in_specs=[VMEM] * 6,
+        out_shape=shape(COL, 8, 512),
+        in_specs=[VMEM] * 5,
         out_specs=VMEM,
+        compiler_params=small(8),
+        cost_estimate=pl.CostEstimate(flops=10**10, bytes_accessed=10**7, transcendentals=0),
         name="first",
-    )(z, const(straight, bf16), const(swapped, bf16), const(qc, f32), const(qs, f32), const(pt, f32))
+    )(z, straight, swapped, cos, sin)
     v = lax.all_to_all(o, "col", split_axis=0, concat_axis=0, tiled=True)
     s = pl.pallas_call(
         second_kernel,
-        out_shape=jax.ShapeDtypeStruct((4 * ROW, 128), bf16),
+        out_shape=shape(4 * ROW, 128),
         in_specs=[VMEM] * 2,
         out_specs=VMEM,
         scratch_shapes=[pltpu.VMEM((4 * ROW, 128), f32)],
+        compiler_params=small(8),
+        cost_estimate=pl.CostEstimate(flops=10**10, bytes_accessed=10**7, transcendentals=0),
         name="second",
-    )(v.reshape(2 * LEN2, 512), const(second_table(), bf16))
+    )(v.reshape(2 * LEN2, 512), const(second_table()))
     x = lax.all_to_all(s, "row", split_axis=0, concat_axis=0, tiled=True)
     out = pl.pallas_call(
         final_kernel,
-        out_shape=jax.ShapeDtypeStruct((SEQS * 16, D), bf16),
-        in_specs=[VMEM, VMEM, ANY],
+        out_shape=shape(SEQS * 16, D),
+        in_specs=[VMEM] * 3,
         out_specs=VMEM,
-        scratch_shapes=[pltpu.VMEM((F, D), bf16), pltpu.SemaphoreType.DMA((OUT_CHUNKS,))],
+        compiler_params=small(16),
         name="final",
-    )(x, const(order_table(), bf16), w_mix_out)
+    )(x, const(order_table()), w_mix_out)
     return out.reshape(SEQS, 1, 16, D)
 
 

time: 85.3 us -> 73.5 us (0.86)
  Pallas kernels: 14.1 us -> 5.65 us
  blocking collectives: 69.5 us -> 67.6 us
  local copies, waits for them, and re-layouts: 1.29 us -> 0.01 us
    pallas_call x4, Pallas kernels: 14.1 us -> 5.65 us  [the longest x1 3.19 us: body(): pl.pallas_call(front_kernel, out_shape=[shape(ROW * A, 128), shape(2 * LE...]
    all_to_all x1, blocking collectives: 16.5 us -> 15.3 us  [body(): x = lax.all_to_all(s, 'row', split_axis=0, concat_axis=0, tiled=True)]
    reshape x1 -> x0, local copies, waits for them, and re-layouts: 1.29 us -> none  [body(): norm_gain.reshape(1, D)]
where the time goes in v2:
time: 73.5 us; the launch traced here: 73.3 us
  blocking collectives  67.6 us (92%)
  Pallas kernels  5.65 us (8%)
    all_to_all x1, blocking collectives, body(): z = lax.all_to_all(y, 'row', split_axis=0, concat_axis=0, tiled=True)  34.8 us
    all_to_all x1, blocking collectives, body(): v = lax.all_to_all(o, 'col', split_axis=0, concat_axis=0, tiled=True)  17.6 us
    all_to_all x1, blocking collectives, body(): x = lax.all_to_all(s, 'row', split_axis=0, concat_axis=0, tiled=True)  15.3 us
    pallas_call x1, Pallas kernels, body(): pl.pallas_call(front_kernel, out_shape=[shape(ROW * A, 128), shape(2 * LE...  3.19 us
    pallas_call x1, Pallas kernels, body(): pl.pallas_call(final_kernel, out_shape=shape(SEQS * 16, D), in_specs=[VME...  1.68 us

profile of v2, /device:TPU:1, one launch (start us, length us, event | category | flops | bytes accessed | tf_op | source)
XLA Modules:
  0.0 73.3 jit_solution(15473866579520144750)
XLA Ops:
  0.0 3.2 %front.1 = (bf16[256,128]{1,0:T(8,128)(2,1)S(1)}, f32[512,128]{1,0:T(8,128)S(1)}, f32[512,128]{1,0:T(8,128)S(1)}, bf16[512,256]{1,0:T(8,128)(2,1)S(1)}, bf16[512,256]{1,0:T(8,128)(2,1)S(1)}) custom-call(bf16[2,4,4,2048]{3,2,1,0:T(4,128)(2,1)} %x_hbm.1, bf16[2048]{0:T(1024)(128)(2,1)} %gain_hbm.1, bf16[128,128]{1,0:T(8,128)(2,1)} %constant.10.clone.table_hbm, ...), custom_call_target="tpu_custom_call" | custom-call | tf_op jit(solution)/shard_map/front/pallas_call | solution.py:220
  3.2 34.8 %all_to_all.27 = bf16[64,4,128]{2,1,0:T(4,128)(2,1)S(1)} all-to-all(bf16[64,4,128]{2,1,0:T(4,128)(2,1)S(1)} %bitcast.10), channel_id=1, replica_groups=mesh['row'=64,'col'=16] {'row'}, dimensions={0} | all-to-all | bytes 131072 | tf_op jit(solution)/shard_map/all_to_all | solution.py:251
  38.0 0.0 copy-start.2
  38.0 0.4 first.1
  38.5 17.6 %all_to_all.28 = bf16[16,8,512]{2,1,0:T(8,128)(2,1)S(1)} all-to-all(bf16[16,8,512]{2,1,0:T(8,128)(2,1)S(1)} %first.1), channel_id=1, replica_groups=mesh['row'=64,'col'=16] {'col'}, dimensions={0} | all-to-all | bytes 262144 | tf_op jit(solution)/shard_map/all_to_all | solution.py:261
  56.0 0.0 copy-done.2
  56.0 0.0 copy-start
  56.0 0.0 copy-start.1
  56.0 0.3 second.1
  56.4 15.3 %all_to_all.29 = bf16[64,4,128]{2,1,0:T(4,128)(2,1)S(1)} all-to-all(bf16[64,4,128]{2,1,0:T(4,128)(2,1)S(1)} %bitcast.12), channel_id=1, replica_groups=mesh['row'=64,'col'=16] {'row'}, dimensions={0} | all-to-all | bytes 131072 | tf_op jit(solution)/shard_map/all_to_all | solution.py:272
  71.6 0.0 copy-done
  71.6 0.0 copy-done.1
  71.6 1.7 %final.1 = bf16[32,2048]{1,0:T(8,128)(2,1)} custom-call(bf16[256,128]{1,0:T(8,128)(2,1)S(1)} %bitcast.8, bf16[256,256]{1,0:T(8,128)(2,1)S(1)} %copy-done.1, bf16[1024,2048]{1,0:T(8,128)(2,1)S(1)} %copy-done), custom_call_target="tpu_custom_call" | custom-call | tf_op jit(solution)/shard_map/final/pallas_call | solution.py:273
Async XLA Ops:
  38.0 18.0 %copy-start.2 = (bf16[128,128]{1,0:T(8,128)(2,1)S(1)}, bf16[128,128]{1,0:T(8,128)(2,1)}, u32[]{:S(2)}) copy-start(bf16[128,128]{1,0:T(8,128)(2,1)} %constant.13.clone.table_ref) | copy-start | bytes 98308
  56.0 15.6 %copy-start = (bf16[1024,2048]{1,0:T(8,128)(2,1)S(1)}, bf16[1024,2048]{1,0:T(8,128)(2,1)}, u32[]{:S(2)}) copy-start(bf16[1024,2048]{1,0:T(8,128)(2,1)} %w_ref.1) | copy-start | bytes 12582916
  56.0 15.6 %copy-start.1 = (bf16[256,256]{1,0:T(8,128)(2,1)S(1)}, bf16[256,256]{1,0:T(8,128)(2,1)}, u32[]{:S(2)}) copy-start(bf16[256,256]{1,0:T(8,128)(2,1)} %constant.14.clone.order_ref) | copy-start | bytes 393220

commit v3 on v2

--- a/solution.py
+++ b/solution.py
@@ -21,7 +21,7 @@
 LEN2 = COL * B
 LENGTH = LEN1 * LEN2
 EPS = 1e-06
-IN_CHUNKS = 4
+IN_CHUNKS = 8
 OUT_CHUNKS = 8
 bf16 = jnp.bfloat16
 f32 = jnp.float32
@@ -83,18 +83,18 @@
     y_ref, cos_ref, sin_ref, straight_ref, swapped_ref,
     x_ref, gain_ref, table_ref, w_ref, rows_ref, send_ref, sems, w_sems,
 ):
-    width = F // IN_CHUNKS
+    depth = D // IN_CHUNKS
     x_copy = pltpu.make_async_copy(x_hbm, x_ref, sems.at[0])
     x_copy.start()
     gain_copy = pltpu.make_async_copy(gain_hbm, gain_ref, sems.at[4])
     gain_copy.start()
+    table_copy = pltpu.make_async_copy(table_hbm, table_ref, sems.at[1])
+    table_copy.start()
     copies = []
     for i in range(IN_CHUNKS):
-        cols = pl.ds(i * width, width)
-        copies.append(pltpu.make_async_copy(w_hbm.at[:, cols], w_ref.at[:, cols], w_sems.at[i]))
+        part = pl.ds(i * depth, depth)
+        copies.append(pltpu.make_async_copy(w_hbm.at[part], w_ref.at[part], w_sems.at[i]))
         copies[-1].start()
-    table_copy = pltpu.make_async_copy(table_hbm, table_ref, sems.at[1])
-    table_copy.start()
     others = [
         pltpu.make_async_copy(straight_hbm, straight_ref, sems.at[2]),
         pltpu.make_async_copy(swapped_hbm, swapped_ref, sems.at[3]),
@@ -114,23 +114,27 @@
     gain_copy.wait()
     gain = gain_ref[...].astype(f32).reshape(1, D)
     normed = (x * lax.rsqrt(mean_square + EPS) * gain).astype(bf16)
-    parts = []
+    mixed = jnp.zeros((32, F), f32)
     for i in range(IN_CHUNKS):
         copies[i].wait()
-        parts.append(jnp.dot(normed, w_ref[:, i * width : (i + 1) * width], preferred_element_type=f32))
-    per = width // G
+        part = slice(i * depth, (i + 1) * depth)
+        mixed += jnp.dot(normed[:, part], w_ref[part, :], preferred_element_type=f32)
     table_copy.wait()
     table = table_ref[...]
     lane = lax.broadcasted_iota(jnp.int32, (ROW, 128), 1)
     first = (lane // 8) % 2 == 0
-    for a in range(A):
+    for pair in range(A // 2):
         blocks = []
-        for g in range(GROUPS):
-            block = parts[g // per][8 * a : 8 * a + 8, (g % per) * G : (g % per + 1) * G]
-            blocks += [block, block]
+        for a in (2 * pair, 2 * pair + 1):
+            for g in range(GROUPS):
+                block = mixed[8 * a : 8 * a + 8, g * G : (g + 1) * G]
+                blocks += [block, block]
         stacked = jnp.concatenate(blocks, 0).astype(bf16)
         both = lax.dot_general(table, stacked, (((1,), (1,)), ((), ())), preferred_element_type=f32)
-        send_ref[pl.ds(a, ROW, stride=A), :] = jnp.where(first, both[:ROW], both[ROW:]) * (1 / math.sqrt(G))
+        for i in range(2):
+            lanes = slice(128 * i, 128 * (i + 1))
+            picked = jnp.where(first, both[:ROW, lanes], both[ROW:, lanes]) * (1 / math.sqrt(G))
+            send_ref[pl.ds(2 * pair + i, ROW, stride=A), :] = picked
     y_ref[...] = send_ref[...].astype(bf16)
     for copy in others:
         copy.wait()
@@ -212,12 +216,13 @@
     return jax.ShapeDtypeStruct(dims, kind)
 
 
-def body(tokens, norm_gain, w_mix_in, w_mix_out):
-    def const(x):
-        return jnp.asarray(x.astype(bf16))
-
+def const(x):
+    return jnp.asarray(x.astype(bf16))
+
+
+def front(tokens, norm_gain, w_mix_in):
     straight, swapped = first_tables()
-    y, cos, sin, straight, swapped = pl.pallas_call(
+    return pl.pallas_call(
         front_kernel,
         out_shape=[
             shape(ROW * A, 128),
@@ -248,8 +253,10 @@
         in_hbm(const(straight)),
         in_hbm(const(swapped)),
     )
-    z = lax.all_to_all(y, "row", split_axis=0, concat_axis=0, tiled=True)
-    o = pl.pallas_call(
+
+
+def first(z, straight, swapped, cos, sin):
+    return pl.pallas_call(
         first_kernel,
         out_shape=shape(COL, 8, 512),
         in_specs=[VMEM] * 5,
@@ -258,8 +265,10 @@
         cost_estimate=pl.CostEstimate(flops=10**10, bytes_accessed=10**7, transcendentals=0),
         name="first",
     )(z, straight, swapped, cos, sin)
-    v = lax.all_to_all(o, "col", split_axis=0, concat_axis=0, tiled=True)
-    s = pl.pallas_call(
+
+
+def second(v):
+    return pl.pallas_call(
         second_kernel,
         out_shape=shape(4 * ROW, 128),
         in_specs=[VMEM] * 2,
@@ -268,9 +277,11 @@
         compiler_params=small(8),
         cost_estimate=pl.CostEstimate(flops=10**10, bytes_accessed=10**7, transcendentals=0),
         name="second",
-    )(v.reshape(2 * LEN2, 512), const(second_table()))
-    x = lax.all_to_all(s, "row", split_axis=0, concat_axis=0, tiled=True)
-    out = pl.pallas_call(
+    )(v, const(second_table()))
+
+
+def final(x, w_mix_out):
+    return pl.pallas_call(
         final_kernel,
         out_shape=shape(SEQS * 16, D),
         in_specs=[VMEM] * 3,
@@ -278,7 +289,16 @@
         compiler_params=small(16),
         name="final",
     )(x, const(order_table()), w_mix_out)
-    return out.reshape(SEQS, 1, 16, D)
+
+
+def body(tokens, norm_gain, w_mix_in, w_mix_out):
+    y, cos, sin, straight, swapped = front(tokens, norm_gain, w_mix_in)
+    z = lax.all_to_all(y, "row", split_axis=0, concat_axis=0, tiled=True)
+    o = first(z, straight, swapped, cos, sin)
+    v = lax.all_to_all(o, "col", split_axis=0, concat_axis=0, tiled=True)
+    s = second(v.reshape(2 * LEN2, 512))
+    x = lax.all_to_all(s, "row", split_axis=0, concat_axis=0, tiled=True)
+    return final(x, w_mix_out).reshape(SEQS, 1, 16, D)
 
 
 def solution(mesh):

time: 73.5 us -> 73.2 us (level)
  no operation moved by 1% of the time
where the time goes in v3:
time: 73.2 us; the launch traced here: 72.9 us
  blocking collectives  67.6 us (92%)
  Pallas kernels  5.28 us (7%)
    all_to_all x1, blocking collectives, body(): z = lax.all_to_all(y, 'row', split_axis=0, concat_axis=0, tiled=True)  34.8 us
    all_to_all x1, blocking collectives, body(): v = lax.all_to_all(o, 'col', split_axis=0, concat_axis=0, tiled=True)  17.6 us
    all_to_all x1, blocking collectives, body(): x = lax.all_to_all(s, 'row', split_axis=0, concat_axis=0, tiled=True)  15.3 us
    pallas_call x1, Pallas kernels, front(): pl.pallas_call(front_kernel, out_shape=[shape(ROW * A, 128), shape(2 * LE...  2.82 us
    pallas_call x1, Pallas kernels, final(): pl.pallas_call(final_kernel, out_shape=shape(SEQS * 16, D), in_specs=[VME...  1.68 us

profile of v3, /device:TPU:1, one launch (start us, length us, event | category | flops | bytes accessed | tf_op | source)
XLA Modules:
  0.0 72.9 jit_solution(626335059382246951)
XLA Ops:
  0.0 2.8 %front.1 = (bf16[256,128]{1,0:T(8,128)(2,1)S(1)}, f32[512,128]{1,0:T(8,128)S(1)}, f32[512,128]{1,0:T(8,128)S(1)}, bf16[512,256]{1,0:T(8,128)(2,1)S(1)}, bf16[512,256]{1,0:T(8,128)(2,1)S(1)}) custom-call(bf16[2,4,4,2048]{3,2,1,0:T(4,128)(2,1)} %x_hbm.1, bf16[2048]{0:T(1024)(128)(2,1)} %gain_hbm.1, bf16[128,128]{1,0:T(8,128)(2,1)} %constant.10.clone.table_hbm, ...), custom_call_target="tpu_custom_call" | custom-call | tf_op jit(solution)/shard_map/front/pallas_call | solution.py:225
  2.8 34.8 %all_to_all.27 = bf16[64,4,128]{2,1,0:T(4,128)(2,1)S(1)} all-to-all(bf16[64,4,128]{2,1,0:T(4,128)(2,1)S(1)} %bitcast.10), channel_id=1, replica_groups=mesh['row'=64,'col'=16] {'row'}, dimensions={0} | all-to-all | bytes 131072 | tf_op jit(solution)/shard_map/all_to_all | solution.py:296
  37.7 0.0 copy-start.2
  37.7 0.4 first.1
  38.1 17.6 %all_to_all.28 = bf16[16,8,512]{2,1,0:T(8,128)(2,1)S(1)} all-to-all(bf16[16,8,512]{2,1,0:T(8,128)(2,1)S(1)} %first.1), channel_id=1, replica_groups=mesh['row'=64,'col'=16] {'col'}, dimensions={0} | all-to-all | bytes 262144 | tf_op jit(solution)/shard_map/all_to_all | solution.py:298
  55.7 0.0 copy-done.2
  55.7 0.0 copy-start
  55.7 0.0 copy-start.1
  55.7 0.3 second.1
  56.0 15.3 %all_to_all.29 = bf16[64,4,128]{2,1,0:T(4,128)(2,1)S(1)} all-to-all(bf16[64,4,128]{2,1,0:T(4,128)(2,1)S(1)} %bitcast.12), channel_id=1, replica_groups=mesh['row'=64,'col'=16] {'row'}, dimensions={0} | all-to-all | bytes 131072 | tf_op jit(solution)/shard_map/all_to_all | solution.py:300
  71.3 0.0 copy-done
  71.3 0.0 copy-done.1
  71.3 1.7 %final.1 = bf16[32,2048]{1,0:T(8,128)(2,1)} custom-call(bf16[256,128]{1,0:T(8,128)(2,1)S(1)} %bitcast.8, bf16[256,256]{1,0:T(8,128)(2,1)S(1)} %copy-done.1, bf16[1024,2048]{1,0:T(8,128)(2,1)S(1)} %copy-done), custom_call_target="tpu_custom_call" | custom-call | tf_op jit(solution)/shard_map/final/pallas_call | solution.py:284
Async XLA Ops:
  37.7 18.0 %copy-start.2 = (bf16[128,128]{1,0:T(8,128)(2,1)S(1)}, bf16[128,128]{1,0:T(8,128)(2,1)}, u32[]{:S(2)}) copy-start(bf16[128,128]{1,0:T(8,128)(2,1)} %constant.13.clone.table_ref) | copy-start | bytes 98308
  55.7 15.6 %copy-start = (bf16[1024,2048]{1,0:T(8,128)(2,1)S(1)}, bf16[1024,2048]{1,0:T(8,128)(2,1)}, u32[]{:S(2)}) copy-start(bf16[1024,2048]{1,0:T(8,128)(2,1)} %w_ref.1) | copy-start | bytes 12582916
  55.7 15.6 %copy-start.1 = (bf16[256,256]{1,0:T(8,128)(2,1)S(1)}, bf16[256,256]{1,0:T(8,128)(2,1)}, u32[]{:S(2)}) copy-start(bf16[256,256]{1,0:T(8,128)(2,1)} %constant.14.clone.order_ref) | copy-start | bytes 393220

commit v4 on v3

--- a/solution.py
+++ b/solution.py
@@ -275,7 +275,7 @@
         out_specs=VMEM,
         scratch_shapes=[pltpu.VMEM((4 * ROW, 128), f32)],
         compiler_params=small(8),
-        cost_estimate=pl.CostEstimate(flops=10**10, bytes_accessed=10**7, transcendentals=0),
+        cost_estimate=pl.CostEstimate(flops=10**4, bytes_accessed=10**4, transcendentals=0),
         name="second",
     )(v, const(second_table()))
 

time: 73.2 us -> 73.1 us (level)
  no operation moved by 1% of the time
where the time goes in v4:
time: 73.1 us; the launch traced here: 72.9 us
  blocking collectives  67.6 us (92%)
  Pallas kernels  5.28 us (7%)
    all_to_all x1, blocking collectives, body(): z = lax.all_to_all(y, 'row', split_axis=0, concat_axis=0, tiled=True)  34.8 us
    all_to_all x1, blocking collectives, body(): v = lax.all_to_all(o, 'col', split_axis=0, concat_axis=0, tiled=True)  17.8 us
    all_to_all x1, blocking collectives, body(): x = lax.all_to_all(s, 'row', split_axis=0, concat_axis=0, tiled=True)  15 us
    pallas_call x1, Pallas kernels, front(): pl.pallas_call(front_kernel, out_shape=[shape(ROW * A, 128), shape(2 * LE...  2.82 us
    pallas_call x1, Pallas kernels, final(): pl.pallas_call(final_kernel, out_shape=shape(SEQS * 16, D), in_specs=[VME...  1.68 us

profile of v4, /device:TPU:1, one launch (start us, length us, event | category | flops | bytes accessed | tf_op | source)
XLA Modules:
  0.0 72.9 jit_solution(3612267510724581843)
XLA Ops:
  0.0 2.8 %front.1 = (bf16[256,128]{1,0:T(8,128)(2,1)S(1)}, f32[512,128]{1,0:T(8,128)S(1)}, f32[512,128]{1,0:T(8,128)S(1)}, bf16[512,256]{1,0:T(8,128)(2,1)S(1)}, bf16[512,256]{1,0:T(8,128)(2,1)S(1)}) custom-call(bf16[2,4,4,2048]{3,2,1,0:T(4,128)(2,1)} %x_hbm.1, bf16[2048]{0:T(1024)(128)(2,1)} %gain_hbm.1, bf16[128,128]{1,0:T(8,128)(2,1)} %constant.10.clone.table_hbm, ...), custom_call_target="tpu_custom_call" | custom-call | tf_op jit(solution)/shard_map/front/pallas_call | solution.py:225
  2.8 34.8 %all_to_all.27 = bf16[64,4,128]{2,1,0:T(4,128)(2,1)S(1)} all-to-all(bf16[64,4,128]{2,1,0:T(4,128)(2,1)S(1)} %bitcast.11), channel_id=1, replica_groups=mesh['row'=64,'col'=16] {'row'}, dimensions={0} | all-to-all | bytes 131072 | tf_op jit(solution)/shard_map/all_to_all | solution.py:296
  37.7 0.0 copy-start.2
  37.7 0.0 copy-start
  37.7 0.0 copy-start.1
  37.7 0.4 first.1
  38.1 17.8 %all_to_all.28 = bf16[16,8,512]{2,1,0:T(8,128)(2,1)S(1)} all-to-all(bf16[16,8,512]{2,1,0:T(8,128)(2,1)S(1)} %first.1), channel_id=1, replica_groups=mesh['row'=64,'col'=16] {'col'}, dimensions={0} | all-to-all | bytes 262144 | tf_op jit(solution)/shard_map/all_to_all | solution.py:298
  55.9 0.0 copy-done.2
  55.9 0.3 second.1
  56.3 15.0 %all_to_all.29 = bf16[64,4,128]{2,1,0:T(4,128)(2,1)S(1)} all-to-all(bf16[64,4,128]{2,1,0:T(4,128)(2,1)S(1)} %bitcast.10), channel_id=1, replica_groups=mesh['row'=64,'col'=16] {'row'}, dimensions={0} | all-to-all | bytes 131072 | tf_op jit(solution)/shard_map/all_to_all | solution.py:300
  71.2 0.0 copy-done
  71.2 0.0 copy-done.1
  71.2 1.7 %final.1 = bf16[32,2048]{1,0:T(8,128)(2,1)} custom-call(bf16[256,128]{1,0:T(8,128)(2,1)S(1)} %bitcast.9, bf16[256,256]{1,0:T(8,128)(2,1)S(1)} %copy-done.1, bf16[1024,2048]{1,0:T(8,128)(2,1)S(1)} %copy-done), custom_call_target="tpu_custom_call" | custom-call | tf_op jit(solution)/shard_map/final/pallas_call | solution.py:284
Async XLA Ops:
  37.7 18.3 %copy-start.2 = (bf16[128,128]{1,0:T(8,128)(2,1)S(1)}, bf16[128,128]{1,0:T(8,128)(2,1)}, u32[]{:S(2)}) copy-start(bf16[128,128]{1,0:T(8,128)(2,1)} %constant.13.clone.table_ref) | copy-start | bytes 98308
  37.7 33.6 %copy-start = (bf16[1024,2048]{1,0:T(8,128)(2,1)S(1)}, bf16[1024,2048]{1,0:T(8,128)(2,1)}, u32[]{:S(2)}) copy-start(bf16[1024,2048]{1,0:T(8,128)(2,1)} %w_ref.1) | copy-start | bytes 12582916
  37.7 33.6 %copy-start.1 = (bf16[256,256]{1,0:T(8,128)(2,1)S(1)}, bf16[256,256]{1,0:T(8,128)(2,1)}, u32[]{:S(2)}) copy-start(bf16[256,256]{1,0:T(8,128)(2,1)} %constant.14.clone.order_ref) | copy-start | bytes 393220

commit v5 on v3

--- a/solution.py
+++ b/solution.py
@@ -110,15 +110,16 @@
         for s in range(SEQS):
             rows_ref[pl.ds(8 * a + 4 * s, 4), :] = x_ref[s, a].astype(f32)
     x = rows_ref[...]
-    mean_square = jnp.mean(x * x, axis=-1, keepdims=True)
     gain_copy.wait()
     gain = gain_ref[...].astype(f32).reshape(1, D)
-    normed = (x * lax.rsqrt(mean_square + EPS) * gain).astype(bf16)
+    gained = (x * gain).astype(bf16)
+    scale = lax.rsqrt(jnp.mean(x * x, axis=-1, keepdims=True) + EPS)
     mixed = jnp.zeros((32, F), f32)
     for i in range(IN_CHUNKS):
         copies[i].wait()
         part = slice(i * depth, (i + 1) * depth)
-        mixed += jnp.dot(normed[:, part], w_ref[part, :], preferred_element_type=f32)
+        mixed += jnp.dot(gained[:, part], w_ref[part, :], preferred_element_type=f32)
+    mixed = mixed * scale
     table_copy.wait()
     table = table_ref[...]
     lane = lax.broadcasted_iota(jnp.int32, (ROW, 128), 1)
@@ -143,9 +144,12 @@
 def swap_sublane_lane(x, sub, lane_step):
     row_bit = (lax.broadcasted_iota(jnp.int32, x.shape, 1) // sub) % 2
     lane_bit = (lax.broadcasted_iota(jnp.int32, x.shape, 2) // lane_step) % 2
-    up = pltpu.roll(pltpu.roll(x, 8 - sub, 1), lane_step, 2)
-    down = pltpu.roll(pltpu.roll(x, sub, 1), 128 - lane_step, 2)
-    return jnp.where(row_bit == lane_bit, x, jnp.where(lane_bit == 1, up, down))
+    partner = jnp.where(lane_bit == 1, pltpu.roll(x, lane_step, 2), pltpu.roll(x, 128 - lane_step, 2))
+    if sub == 4:
+        partner = pltpu.roll(partner, 4, 1)
+    else:
+        partner = jnp.where(row_bit == 0, pltpu.roll(partner, 8 - sub, 1), pltpu.roll(partner, sub, 1))
+    return jnp.where(row_bit == lane_bit, x, partner)
 
 
 def first_kernel(z_ref, straight_ref, swapped_ref, cos_ref, sin_ref, o_ref):

time: 73.2 us -> 73.2 us (level)
  no operation moved by 1% of the time
where the time goes in v5:
time: 73.2 us; the launch traced here: 73 us
  blocking collectives  67.6 us (92%)
  Pallas kernels  5.29 us (7%)
    all_to_all x1, blocking collectives, body(): z = lax.all_to_all(y, 'row', split_axis=0, concat_axis=0, tiled=True)  34.8 us
    all_to_all x1, blocking collectives, body(): v = lax.all_to_all(o, 'col', split_axis=0, concat_axis=0, tiled=True)  17.6 us
    all_to_all x1, blocking collectives, body(): x = lax.all_to_all(s, 'row', split_axis=0, concat_axis=0, tiled=True)  15.3 us
    pallas_call x1, Pallas kernels, front(): pl.pallas_call(front_kernel, out_shape=[shape(ROW * A, 128), shape(2 * LE...  2.82 us
    pallas_call x1, Pallas kernels, final(): pl.pallas_call(final_kernel, out_shape=shape(SEQS * 16, D), in_specs=[VME...  1.68 us

profile of v5, /device:TPU:1, one launch (start us, length us, event | category | flops | bytes accessed | tf_op | source)
XLA Modules:
  0.0 73.0 jit_solution(12116857832201624004)
XLA Ops:
  0.0 2.8 %front.1 = (bf16[256,128]{1,0:T(8,128)(2,1)S(1)}, f32[512,128]{1,0:T(8,128)S(1)}, f32[512,128]{1,0:T(8,128)S(1)}, bf16[512,256]{1,0:T(8,128)(2,1)S(1)}, bf16[512,256]{1,0:T(8,128)(2,1)S(1)}) custom-call(bf16[2,4,4,2048]{3,2,1,0:T(4,128)(2,1)} %x_hbm.1, bf16[2048]{0:T(1024)(128)(2,1)} %gain_hbm.1, bf16[128,128]{1,0:T(8,128)(2,1)} %constant.10.clone.table_hbm, ...), custom_call_target="tpu_custom_call" | custom-call | tf_op jit(solution)/shard_map/front/pallas_call | solution.py:229
  2.8 34.8 %all_to_all.27 = bf16[64,4,128]{2,1,0:T(4,128)(2,1)S(1)} all-to-all(bf16[64,4,128]{2,1,0:T(4,128)(2,1)S(1)} %bitcast.10), channel_id=1, replica_groups=mesh['row'=64,'col'=16] {'row'}, dimensions={0} | all-to-all | bytes 131072 | tf_op jit(solution)/shard_map/all_to_all | solution.py:300
  37.7 0.0 copy-start.2
  37.7 0.4 first.1
  38.1 17.6 %all_to_all.28 = bf16[16,8,512]{2,1,0:T(8,128)(2,1)S(1)} all-to-all(bf16[16,8,512]{2,1,0:T(8,128)(2,1)S(1)} %first.1), channel_id=1, replica_groups=mesh['row'=64,'col'=16] {'col'}, dimensions={0} | all-to-all | bytes 262144 | tf_op jit(solution)/shard_map/all_to_all | solution.py:302
  55.7 0.0 copy-done.2
  55.7 0.0 copy-start
  55.7 0.0 copy-start.1
  55.7 0.3 second.1
  56.0 15.3 %all_to_all.29 = bf16[64,4,128]{2,1,0:T(4,128)(2,1)S(1)} all-to-all(bf16[64,4,128]{2,1,0:T(4,128)(2,1)S(1)} %bitcast.12), channel_id=1, replica_groups=mesh['row'=64,'col'=16] {'row'}, dimensions={0} | all-to-all | bytes 131072 | tf_op jit(solution)/shard_map/all_to_all | solution.py:304
  71.3 0.0 copy-done
  71.3 0.0 copy-done.1
  71.3 1.7 %final.1 = bf16[32,2048]{1,0:T(8,128)(2,1)} custom-call(bf16[256,128]{1,0:T(8,128)(2,1)S(1)} %bitcast.8, bf16[256,256]{1,0:T(8,128)(2,1)S(1)} %copy-done.1, bf16[1024,2048]{1,0:T(8,128)(2,1)S(1)} %copy-done), custom_call_target="tpu_custom_call" | custom-call | tf_op jit(solution)/shard_map/final/pallas_call | solution.py:288
Async XLA Ops:
  37.7 18.0 %copy-start.2 = (bf16[128,128]{1,0:T(8,128)(2,1)S(1)}, bf16[128,128]{1,0:T(8,128)(2,1)}, u32[]{:S(2)}) copy-start(bf16[128,128]{1,0:T(8,128)(2,1)} %constant.13.clone.table_ref) | copy-start | bytes 98308
  55.7 15.6 %copy-start = (bf16[1024,2048]{1,0:T(8,128)(2,1)S(1)}, bf16[1024,2048]{1,0:T(8,128)(2,1)}, u32[]{:S(2)}) copy-start(bf16[1024,2048]{1,0:T(8,128)(2,1)} %w_ref.1) | copy-start | bytes 12582916
  55.7 15.6 %copy-start.1 = (bf16[256,256]{1,0:T(8,128)(2,1)S(1)}, bf16[256,256]{1,0:T(8,128)(2,1)}, u32[]{:S(2)}) copy-start(bf16[256,256]{1,0:T(8,128)(2,1)} %constant.14.clone.order_ref) | copy-start | bytes 393220

commit v6 on v3

--- a/solution.py
+++ b/solution.py
@@ -21,7 +21,8 @@
 LEN2 = COL * B
 LENGTH = LEN1 * LEN2
 EPS = 1e-06
-IN_CHUNKS = 8
+CHUNKS = ((0, 512), (512, 512), (1024, 256), (1280, 256), (1536, 256), (1792, 256))
+IN_CHUNKS = len(CHUNKS)
 OUT_CHUNKS = 8
 bf16 = jnp.bfloat16
 f32 = jnp.float32
@@ -83,7 +84,6 @@
     y_ref, cos_ref, sin_ref, straight_ref, swapped_ref,
     x_ref, gain_ref, table_ref, w_ref, rows_ref, send_ref, sems, w_sems,
 ):
-    depth = D // IN_CHUNKS
     x_copy = pltpu.make_async_copy(x_hbm, x_ref, sems.at[0])
     x_copy.start()
     gain_copy = pltpu.make_async_copy(gain_hbm, gain_ref, sems.at[4])
@@ -92,7 +92,7 @@
     table_copy.start()
     copies = []
     for i in range(IN_CHUNKS):
-        part = pl.ds(i * depth, depth)
+        part = pl.ds(*CHUNKS[i])
         copies.append(pltpu.make_async_copy(w_hbm.at[part], w_ref.at[part], w_sems.at[i]))
         copies[-1].start()
     others = [
@@ -117,7 +117,7 @@
     mixed = jnp.zeros((32, F), f32)
     for i in range(IN_CHUNKS):
         copies[i].wait()
-        part = slice(i * depth, (i + 1) * depth)
+        part = slice(CHUNKS[i][0], sum(CHUNKS[i]))
         mixed += jnp.dot(normed[:, part], w_ref[part, :], preferred_element_type=f32)
     table_copy.wait()
     table = table_ref[...]

time: 73.2 us -> 73.1 us (level)
  no operation moved by 1% of the time
where the time goes in v6:
time: 73.1 us; the launch traced here: 72.9 us
  blocking collectives  67.6 us (92%)
  Pallas kernels  5.26 us (7%)
    all_to_all x1, blocking collectives, body(): z = lax.all_to_all(y, 'row', split_axis=0, concat_axis=0, tiled=True)  34.8 us
    all_to_all x1, blocking collectives, body(): v = lax.all_to_all(o, 'col', split_axis=0, concat_axis=0, tiled=True)  17.6 us
    all_to_all x1, blocking collectives, body(): x = lax.all_to_all(s, 'row', split_axis=0, concat_axis=0, tiled=True)  15.2 us
    pallas_call x1, Pallas kernels, front(): pl.pallas_call(front_kernel, out_shape=[shape(ROW * A, 128), shape(2 * LE...  2.8 us
    pallas_call x1, Pallas kernels, final(): pl.pallas_call(final_kernel, out_shape=shape(SEQS * 16, D), in_specs=[VME...  1.68 us

profile of v6, /device:TPU:1, one launch (start us, length us, event | category | flops | bytes accessed | tf_op | source)
XLA Modules:
  0.0 72.9 jit_solution(15288580685644900246)
XLA Ops:
  0.0 2.8 %front.1 = (bf16[256,128]{1,0:T(8,128)(2,1)S(1)}, f32[512,128]{1,0:T(8,128)S(1)}, f32[512,128]{1,0:T(8,128)S(1)}, bf16[512,256]{1,0:T(8,128)(2,1)S(1)}, bf16[512,256]{1,0:T(8,128)(2,1)S(1)}) custom-call(bf16[2,4,4,2048]{3,2,1,0:T(4,128)(2,1)} %x_hbm.1, bf16[2048]{0:T(1024)(128)(2,1)} %gain_hbm.1, bf16[128,128]{1,0:T(8,128)(2,1)} %constant.10.clone.table_hbm, ...), custom_call_target="tpu_custom_call" | custom-call | tf_op jit(solution)/shard_map/front/pallas_call | solution.py:225
  2.8 34.8 %all_to_all.27 = bf16[64,4,128]{2,1,0:T(4,128)(2,1)S(1)} all-to-all(bf16[64,4,128]{2,1,0:T(4,128)(2,1)S(1)} %bitcast.10), channel_id=1, replica_groups=mesh['row'=64,'col'=16] {'row'}, dimensions={0} | all-to-all | bytes 131072 | tf_op jit(solution)/shard_map/all_to_all | solution.py:296
  37.6 0.0 copy-start.2
  37.6 0.4 first.1
  38.1 17.6 %all_to_all.28 = bf16[16,8,512]{2,1,0:T(8,128)(2,1)S(1)} all-to-all(bf16[16,8,512]{2,1,0:T(8,128)(2,1)S(1)} %first.1), channel_id=1, replica_groups=mesh['row'=64,'col'=16] {'col'}, dimensions={0} | all-to-all | bytes 262144 | tf_op jit(solution)/shard_map/all_to_all | solution.py:298
  55.6 0.0 copy-done.2
  55.6 0.0 copy-start
  55.6 0.0 copy-start.1
  55.6 0.3 second.1
  56.0 15.2 %all_to_all.29 = bf16[64,4,128]{2,1,0:T(4,128)(2,1)S(1)} all-to-all(bf16[64,4,128]{2,1,0:T(4,128)(2,1)S(1)} %bitcast.12), channel_id=1, replica_groups=mesh['row'=64,'col'=16] {'row'}, dimensions={0} | all-to-all | bytes 131072 | tf_op jit(solution)/shard_map/all_to_all | solution.py:300
  71.2 0.0 copy-done
  71.2 0.0 copy-done.1
  71.2 1.7 %final.1 = bf16[32,2048]{1,0:T(8,128)(2,1)} custom-call(bf16[256,128]{1,0:T(8,128)(2,1)S(1)} %bitcast.8, bf16[256,256]{1,0:T(8,128)(2,1)S(1)} %copy-done.1, bf16[1024,2048]{1,0:T(8,128)(2,1)S(1)} %copy-done), custom_call_target="tpu_custom_call" | custom-call | tf_op jit(solution)/shard_map/final/pallas_call | solution.py:284
Async XLA Ops:
  37.6 18.0 %copy-start.2 = (bf16[128,128]{1,0:T(8,128)(2,1)S(1)}, bf16[128,128]{1,0:T(8,128)(2,1)}, u32[]{:S(2)}) copy-start(bf16[128,128]{1,0:T(8,128)(2,1)} %constant.13.clone.table_ref) | copy-start | bytes 98308
  55.6 15.6 %copy-start = (bf16[1024,2048]{1,0:T(8,128)(2,1)S(1)}, bf16[1024,2048]{1,0:T(8,128)(2,1)}, u32[]{:S(2)}) copy-start(bf16[1024,2048]{1,0:T(8,128)(2,1)} %w_ref.1) | copy-start | bytes 12582916
  55.6 15.6 %copy-start.1 = (bf16[256,256]{1,0:T(8,128)(2,1)S(1)}, bf16[256,256]{1,0:T(8,128)(2,1)}, u32[]{:S(2)}) copy-start(bf16[256,256]{1,0:T(8,128)(2,1)} %constant.14.clone.order_ref) | copy-start | bytes 393220

commit v7 on v4

--- a/solution.py
+++ b/solution.py
@@ -262,7 +262,7 @@
         in_specs=[VMEM] * 5,
         out_specs=VMEM,
         compiler_params=small(8),
-        cost_estimate=pl.CostEstimate(flops=10**10, bytes_accessed=10**7, transcendentals=0),
+        cost_estimate=pl.CostEstimate(flops=10**9, bytes_accessed=10**7, transcendentals=0),
         name="first",
     )(z, straight, swapped, cos, sin)
 

time: 73.1 us -> 73 us (level)
  no operation moved by 1% of the time
where the time goes in v7:
time: 73 us; the launch traced here: 72.8 us
  blocking collectives  67.4 us (92%)
  Pallas kernels  5.42 us (7%)
    all_to_all x1, blocking collectives, body(): z = lax.all_to_all(y, 'row', split_axis=0, concat_axis=0, tiled=True)  34.8 us
    all_to_all x1, blocking collectives, body(): v = lax.all_to_all(o, 'col', split_axis=0, concat_axis=0, tiled=True)  17.6 us
    all_to_all x1, blocking collectives, body(): x = lax.all_to_all(s, 'row', split_axis=0, concat_axis=0, tiled=True)  15 us
    pallas_call x1, Pallas kernels, front(): pl.pallas_call(front_kernel, out_shape=[shape(ROW * A, 128), shape(2 * LE...  2.96 us
    pallas_call x1, Pallas kernels, final(): pl.pallas_call(final_kernel, out_shape=shape(SEQS * 16, D), in_specs=[VME...  1.68 us

profile of v7, /device:TPU:1, one launch (start us, length us, event | category | flops | bytes accessed | tf_op | source)
XLA Modules:
  0.0 72.8 jit_solution(17773373256997983454)
XLA Ops:
  0.0 0.0 copy-start.2
  0.0 0.0 copy-start.1
  0.0 0.0 copy-start
  0.0 3.0 %front.1 = (bf16[256,128]{1,0:T(8,128)(2,1)S(1)}, f32[512,128]{1,0:T(8,128)S(1)}, f32[512,128]{1,0:T(8,128)S(1)}, bf16[512,256]{1,0:T(8,128)(2,1)S(1)}, bf16[512,256]{1,0:T(8,128)(2,1)S(1)}) custom-call(bf16[2,4,4,2048]{3,2,1,0:T(4,128)(2,1)} %x_hbm.1, bf16[2048]{0:T(1024)(128)(2,1)} %gain_hbm.1, bf16[128,128]{1,0:T(8,128)(2,1)} %constant.10.clone.table_hbm, ...), custom_call_target="tpu_custom_call" | custom-call | tf_op jit(solution)/shard_map/front/pallas_call | solution.py:225
  3.0 34.8 %all_to_all.27 = bf16[64,4,128]{2,1,0:T(4,128)(2,1)S(1)} all-to-all(bf16[64,4,128]{2,1,0:T(4,128)(2,1)S(1)} %bitcast.11), channel_id=1, replica_groups=mesh['row'=64,'col'=16] {'row'}, dimensions={0} | all-to-all | bytes 131072 | tf_op jit(solution)/shard_map/all_to_all | solution.py:296
  37.8 0.4 first.1
  38.2 17.6 %all_to_all.28 = bf16[16,8,512]{2,1,0:T(8,128)(2,1)S(1)} all-to-all(bf16[16,8,512]{2,1,0:T(8,128)(2,1)S(1)} %first.1), channel_id=1, replica_groups=mesh['row'=64,'col'=16] {'col'}, dimensions={0} | all-to-all | bytes 262144 | tf_op jit(solution)/shard_map/all_to_all | solution.py:298
  55.8 0.0 copy-done.2
  55.8 0.3 second.1
  56.2 15.0 %all_to_all.29 = bf16[64,4,128]{2,1,0:T(4,128)(2,1)S(1)} all-to-all(bf16[64,4,128]{2,1,0:T(4,128)(2,1)S(1)} %bitcast.10), channel_id=1, replica_groups=mesh['row'=64,'col'=16] {'row'}, dimensions={0} | all-to-all | bytes 131072 | tf_op jit(solution)/shard_map/all_to_all | solution.py:300
  71.1 0.0 copy-done.1
  71.1 0.0 copy-done
  71.1 1.7 %final.1 = bf16[32,2048]{1,0:T(8,128)(2,1)} custom-call(bf16[256,128]{1,0:T(8,128)(2,1)S(1)} %bitcast.9, bf16[256,256]{1,0:T(8,128)(2,1)S(1)} %copy-done.1, bf16[1024,2048]{1,0:T(8,128)(2,1)S(1)} %copy-done), custom_call_target="tpu_custom_call" | custom-call | tf_op jit(solution)/shard_map/final/pallas_call | solution.py:284
Async XLA Ops:
  0.0 55.8 %copy-start.2 = (bf16[128,128]{1,0:T(8,128)(2,1)S(1)}, bf16[128,128]{1,0:T(8,128)(2,1)}, u32[]{:S(2)}) copy-start(bf16[128,128]{1,0:T(8,128)(2,1)} %constant.13.clone.table_ref) | copy-start | bytes 98308
  0.0 71.1 %copy-start.1 = (bf16[256,256]{1,0:T(8,128)(2,1)S(1)}, bf16[256,256]{1,0:T(8,128)(2,1)}, u32[]{:S(2)}) copy-start(bf16[256,256]{1,0:T(8,128)(2,1)} %constant.14.clone.order_ref) | copy-start | bytes 393220
  0.0 71.1 %copy-start = (bf16[1024,2048]{1,0:T(8,128)(2,1)S(1)}, bf16[1024,2048]{1,0:T(8,128)(2,1)}, u32[]{:S(2)}) copy-start(bf16[1024,2048]{1,0:T(8,128)(2,1)} %w_ref.1) | copy-start | bytes 12582916
